TPU v7x, 32 devices: a whole 2x2x4 slice. The times are simulated.
32 devices in a mesh: fs: 8 (over z, y), tp: 4 (over x, core).
Axes of the slice: x: 2, y: 2, z: 4, core: 2. Of those that a mesh axis runs over, the one named last changes fastest.
Arguments:
- stream: bfloat16 [4096, 1024], P(('fs', 'tp')), may hold values from -3 to 3
- mixer_out: bfloat16 [4096, 1024], P(('fs', 'tp')), may hold values from -6 to 6
- ffn_gains: float32 [4, 1024], replicated, may hold values from 0.5 to 1.5
- mixer_gain: float32 [1024], replicated, may hold values from 0.25 to 0.6
- gate_first: bfloat16 [1024, 2816], P('fs', 'tp'), may hold values from -0.1875 to 0.1875
- up_first: bfloat16 [1024, 2816], P('fs', 'tp'), may hold values from -0.1875 to 0.1875
- down_first: bfloat16 [2816, 1024], P('tp', 'fs'), may hold values from -0.109375 to 0.109375
- gate_second: bfloat16 [1024, 2816], P('fs', 'tp'), may hold values from -0.1875 to 0.1875
- up_second: bfloat16 [1024, 2816], P('fs', 'tp'), may hold values from -0.1875 to 0.1875
- down_second: bfloat16 [2816, 1024], P('tp', 'fs'), may hold values from -0.109375 to 0.109375
Outputs:
- layer_out: bfloat16 [4096, 1024], P(('fs', 'tp'))
All inputs are finite; a program needn't handle non-finite values.
Results may differ from a plain program's by a relative error of at most 0.02.
Values may be sent and summed in bfloat16 or wider, within the bound.
A program may use at most 64 MiB of HBM per device.

v0:
```python
import jax
import jax.numpy as jnp
from jax import lax
from jax.sharding import PartitionSpec as P

epsilon = 1e-06
half_weight = 0.5


def over_all(section, axis, dim, apply):
    everything = lax.all_gather(section, axis, axis=dim, tiled=True)
    return apply(everything, jnp.int32(0))


def summed_rows(portion, rows, axis):
    count = rows * lax.axis_size(axis)
    sent = portion(jnp.int32(0), count).astype(jnp.bfloat16)
    return lax.psum_scatter(sent, axis, scatter_dimension=0, tiled=True).astype(jnp.float32)


def rms_rows(values, gain_row):
    widened = values.astype(jnp.float32)
    inverse_rms = lax.rsqrt(jnp.mean(widened * widened, axis=-1, keepdims=True) + epsilon)
    return (widened * inverse_rms * gain_row.astype(jnp.float32)).astype(jnp.bfloat16)


def add_branch(rows, normed_branch, factor):
    return (rows.astype(jnp.float32) + factor * normed_branch.astype(jnp.float32)).astype(
        jnp.bfloat16
    )


def collect_weights(gate_local, up_local, down_local):
    gate_full, up_full = (
        lax.all_gather(gate_local, "fs", axis=0, tiled=True),
        lax.all_gather(up_local, "fs", axis=0, tiled=True),
    )
    down_full = lax.all_gather(down_local, "fs", axis=1, tiled=True)
    return (gate_full, up_full, down_full)


def half_step(rows, gain_pre, gain_post, weight_set):
    gate_full, up_full, down_full = weight_set
    normed = rms_rows(rows, gain_pre)

    def activate(tokens_part, first_row):
        gate_sum = jnp.dot(tokens_part, gate_full, preferred_element_type=jnp.float32)
        up_sum = jnp.dot(tokens_part, up_full, preferred_element_type=jnp.float32)
        return (jax.nn.silu(gate_sum) * up_sum).astype(jnp.bfloat16)

    hidden = over_all(normed, "tp", 0, activate)

    def project(first_row, row_count):
        row_block = lax.dynamic_slice_in_dim(hidden, first_row, row_count, 0)
        return jnp.dot(row_block, down_full, preferred_element_type=jnp.float32)

    branch = summed_rows(project, normed.shape[0], "tp").astype(jnp.bfloat16)
    return add_branch(rows, rms_rows(branch, gain_post), half_weight)


def on_device(
    stream,
    mixer_out,
    ffn_gains,
    mixer_gain,
    gate_first,
    up_first,
    down_first,
    gate_second,
    up_second,
    down_second,
):
    first_set = collect_weights(gate_first, up_first, down_first)
    after_first = half_step(stream, ffn_gains[0], ffn_gains[1], first_set)
    mixed_in = add_branch(after_first, rms_rows(mixer_out, mixer_gain), 1.0)
    second_set = collect_weights(gate_second, up_second, down_second)
    return half_step(mixed_in, ffn_gains[2], ffn_gains[3], second_set)


def solution(mesh):
    in_specs = (
        P(("fs", "tp"), None),
        P(("fs", "tp"), None),
        P(),
        P(),
        P("fs", "tp"),
        P("fs", "tp"),
        P("tp", "fs"),
        P("fs", "tp"),
        P("fs", "tp"),
        P("tp", "fs"),
    )
    out_specs = P(("fs", "tp"), None)
    return jax.shard_map(
        on_device, mesh=mesh, in_specs=in_specs, out_specs=out_specs, check_vma=False
    )
```

profile of v0, /device:TPU:0, one launch (start us, length us, event | category | flops | bytes accessed | tf_op | source)
XLA Modules:
  0.0 382.4 jit_solution(1594553680892777717)
XLA Ops:
  6.5 0.0 all-gather.9.cloned.1.call-start
  6.5 0.9 fusion.23
  7.4 1.1 fusion.13
  8.5 1.8 fusion.15
  10.3 0.0 all-gather.9.cloned.1.call-update
  10.3 0.0 all-gather.11.cloned.1.call-start
  10.4 0.7 all-gather.11.cloned.1.call-update
  11.1 0.0 all-gather.13.cloned.1.call-start
  11.1 0.7 all-gather.13.cloned.1.call-update
  11.8 0.0 all-gather.15.cloned.1.call-start
  11.9 0.5 all-gather.15.cloned.1.call-update
  12.4 0.0 reduce-scatter.3.cloned.1.call-start
  12.4 17.4 %all-gather.9.cloned.1.call-done = bf16[512,1024]{1,0:T(8,128)(2,1)} async-done(((bf16[128,1024]{1,0:T(8,128)(2,1)}), bf16[512,1024]{1,0:T(8,128)(2,1)}) %all-gather.9.cloned.1.call-update) | async-done | bytes 1048592 | tf_op jit(solution)/shard_map/all_gather | solution.py:11
  29.8 45.6 %all-gather.11.cloned.1.call-done = bf16[1024,704]{0,1:T(8,128)(2,1)} async-done(((bf16[128,704]{0,1:T(8,128)(2,1)}), bf16[1024,704]{0,1:T(8,128)(2,1)}) %all-gather.11.cloned.1.call-update) | async-done | bytes 1441808 | tf_op jit(solution)/shard_map/all_gather | solution.py:35
  75.4 2.6 fusion.24
  78.0 0.0 copy-start.1
  78.0 41.6 %all-gather.13.cloned.1.call-done = bf16[1024,704]{0,1:T(8,128)(2,1)} async-done(((bf16[128,704]{0,1:T(8,128)(2,1)}), bf16[1024,704]{0,1:T(8,128)(2,1)}) %all-gather.13.cloned.1.call-update) | async-done | bytes 1441808 | tf_op jit(solution)/shard_map/all_gather | solution.py:36
  119.7 44.1 %all-gather.15.cloned.1.call-done = bf16[704,1024]{1,0:T(8,128)(2,1)} async-done(((bf16[704,128]{1,0:T(8,128)(2,1)}), bf16[704,1024]{1,0:T(8,128)(2,1)}) %all-gather.15.cloned.1.call-update) | async-done | bytes 1441808 | tf_op jit(solution)/shard_map/all_gather | solution.py:38
  163.8 0.0 copy-done.3
  163.8 4.7 %convolution_convert_fusion.1 = bf16[512,1024]{1,0:T(8,128)(2,1)} fusion(bf16[704,1024]{1,0:T(8,128)(2,1)} %all-gather.15.cloned.1.call-done, bf16[512,1024]{1,0:T(8,128)(2,1)S(1)} %copy-done.3, bf16[1024,704]{0,1:T(8,128)(2,1)} %all-gather.13.cloned.1.call-done, f32[512,704]{0,1:T(8,128)S(1)} %fusion.24), kind=kOutput, calls=%fused_computation.1 | convolution fusion | flops 1479081984 | bytes 6422528 | tf_op jit(solution)/shard_map/dot_general | solution.py:55
  168.5 0.0 reduce-scatter.3.cloned.1.call-update
  168.6 0.0 all-gather.19.cloned.1.call-start
  168.6 0.5 all-gather.19.cloned.1.call-update
  169.1 0.0 all-gather.17.cloned.1.call-start
  169.2 0.0 copy-done.1
  169.2 0.1 fusion.7
  169.3 22.8 %reduce-scatter.3.cloned.1.call-done = bf16[128,1024]{1,0:T(8,128)(2,1)} async-done(((bf16[512,1024]{1,0:T(8,128)(2,1)}), bf16[128,1024]{1,0:T(8,128)(2,1)}) %reduce-scatter.3.cloned.1.call-update) | async-done | bytes 262160 | tf_op jit(solution)/shard_map/reduce_scatter | solution.py:18
  192.1 1.1 fusion.4
  193.2 0.0 copy-done
  193.2 0.0 copy-done.2
  193.2 1.3 fusion.17
  194.6 0.8 fusion.19
  195.4 0.0 all-gather.17.cloned.1.call-update
  195.5 0.0 all-gather.21.cloned.1.call-start
  195.5 0.7 all-gather.21.cloned.1.call-update
  196.2 0.0 all-gather.23.cloned.1.call-start
  196.3 0.7 all-gather.23.cloned.1.call-update
  196.9 0.0 reduce-scatter.5.cloned.1.call-start
  197.0 40.5 %all-gather.19.cloned.1.call-done = bf16[1024,704]{0,1:T(8,128)(2,1)} async-done(((bf16[128,704]{0,1:T(8,128)(2,1)}), bf16[1024,704]{0,1:T(8,128)(2,1)}) %all-gather.19.cloned.1.call-update) | async-done | bytes 1441808 | tf_op jit(solution)/shard_map/all_gather | solution.py:35
  237.5 16.9 %all-gather.17.cloned.1.call-done = bf16[512,1024]{1,0:T(8,128)(2,1)} async-done(((bf16[128,1024]{1,0:T(8,128)(2,1)}), bf16[512,1024]{1,0:T(8,128)(2,1)}) %all-gather.17.cloned.1.call-update) | async-done | bytes 1048592 | tf_op jit(solution)/shard_map/all_gather | solution.py:11
  254.4 2.7 fusion.25
  257.2 42.8 %all-gather.21.cloned.1.call-done = bf16[1024,704]{0,1:T(8,128)(2,1)} async-done(((bf16[128,704]{0,1:T(8,128)(2,1)}), bf16[1024,704]{0,1:T(8,128)(2,1)}) %all-gather.21.cloned.1.call-update) | async-done | bytes 1441808 | tf_op jit(solution)/shard_map/all_gather | solution.py:36
  300.0 44.3 %all-gather.23.cloned.1.call-done = bf16[704,1024]{1,0:T(8,128)(2,1)} async-done(((bf16[704,128]{1,0:T(8,128)(2,1)}), bf16[704,1024]{1,0:T(8,128)(2,1)}) %all-gather.23.cloned.1.call-update) | async-done | bytes 1441808 | tf_op jit(solution)/shard_map/all_gather | solution.py:38
  344.3 4.7 %convolution_convert_fusion = bf16[512,1024]{1,0:T(8,128)(2,1)} fusion(bf16[704,1024]{1,0:T(8,128)(2,1)} %all-gather.23.cloned.1.call-done, bf16[512,1024]{1,0:T(8,128)(2,1)S(1)} %copy-done.4, bf16[1024,704]{0,1:T(8,128)(2,1)} %all-gather.21.cloned.1.call-done, f32[512,704]{0,1:T(8,128)S(1)} %fusion.25), kind=kOutput, calls=%fused_computation | convolution fusion | flops 1479081984 | bytes 6422528 | tf_op jit(solution)/shard_map/dot_general | solution.py:55
  349.0 0.0 reduce-scatter.5.cloned.1.call-update
  349.0 23.6 %reduce-scatter.5.cloned.1.call-done = bf16[128,1024]{1,0:T(8,128)(2,1)} async-done(((bf16[512,1024]{1,0:T(8,128)(2,1)}), bf16[128,1024]{1,0:T(8,128)(2,1)}) %reduce-scatter.5.cloned.1.call-update) | async-done | bytes 262160 | tf_op jit(solution)/shard_map/reduce_scatter | solution.py:18
  372.6 1.1 fusion.10
  373.7 1.8 fusion.20
  (10 shorter events, 0.1 us)
Async XLA Ops:
  6.5 23.3 %all-gather.9.cloned.1.call-start = ((), (), s32[]{:S(2)}) async-start(), calls=%async_computation.2 | async-start | bytes 1310720 | tf_op jit(solution)/shard_map/all_gather | solution.py:11
  10.3 65.1 %all-gather.11.cloned.1.call-start = ((), (), s32[]{:S(2)}) async-start(), calls=%async_computation.3 | async-start | bytes 1622016 | tf_op jit(solution)/shard_map/all_gather | solution.py:35
  11.1 108.6 %all-gather.13.cloned.1.call-start = ((), (), s32[]{:S(2)}) async-start(), calls=%async_computation.4 | async-start | bytes 1622016 | tf_op jit(solution)/shard_map/all_gather | solution.py:36
  11.8 152.0 %all-gather.15.cloned.1.call-start = ((), (), s32[]{:S(2)}) async-start(), calls=%async_computation.5 | async-start | bytes 1622016 | tf_op jit(solution)/shard_map/all_gather | solution.py:38
  12.4 179.7 %reduce-scatter.3.cloned.1.call-start = ((), (), s32[]{:S(2)}) async-start(), calls=%async_computation.6 | async-start | bytes 1310720 | tf_op jit(solution)/shard_map/reduce_scatter | solution.py:18
  29.8 134.0 %copy-start.3 = (bf16[512,1024]{1,0:T(8,128)(2,1)S(1)}, bf16[512,1024]{1,0:T(8,128)(2,1)}, u32[]{:S(2)}) copy-start(bf16[512,1024]{1,0:T(8,128)(2,1)} %all-gather.9.cloned.1.call-done) | copy-start | bytes 3145732
  78.0 91.2 %copy-start.1 = (bf16[128,1024]{1,0:T(8,128)(2,1)S(1)}, bf16[128,1024]{1,0:T(8,128)(2,1)}, u32[]{:S(2)}) copy-start(bf16[128,1024]{1,0:T(8,128)(2,1)} %param.11) | copy-start | bytes 786436
  168.5 24.7 %copy-start = (bf16[128,1024]{1,0:T(8,128)(2,1)S(1)}, bf16[128,1024]{1,0:T(8,128)(2,1)}, u32[]{:S(2)}) copy-start(bf16[128,1024]{1,0:T(8,128)(2,1)} %param.10) | copy-start | bytes 786436
  168.5 24.7 %copy-start.2 = (f32[1024]{0:T(1024)S(1)}, f32[1024]{0:T(1024)}, u32[]{:S(2)}) copy-start(f32[1024]{0:T(1024)} %param.13) | copy-start | bytes 12292
  168.6 69.0 %all-gather.19.cloned.1.call-start = ((), (), s32[]{:S(2)}) async-start(), calls=%async_computation.8 | async-start | bytes 1622016 | tf_op jit(solution)/shard_map/all_gather | solution.py:35
  169.1 85.3 %all-gather.17.cloned.1.call-start = ((), (), s32[]{:S(2)}) async-start(), calls=%async_computation.7 | async-start | bytes 1310720 | tf_op jit(solution)/shard_map/all_gather | solution.py:11
  195.5 104.5 %all-gather.21.cloned.1.call-start = ((), (), s32[]{:S(2)}) async-start(), calls=%async_computation.9 | async-start | bytes 1622016 | tf_op jit(solution)/shard_map/all_gather | solution.py:36
  196.2 148.1 %all-gather.23.cloned.1.call-start = ((), (), s32[]{:S(2)}) async-start(), calls=%async_computation.10 | async-start | bytes 1622016 | tf_op jit(solution)/shard_map/all_gather | solution.py:38
  196.9 175.6 %reduce-scatter.5.cloned.1.call-start = ((), (), s32[]{:S(2)}) async-start(), calls=%async_computation.11 | async-start | bytes 1310720 | tf_op jit(solution)/shard_map/reduce_scatter | solution.py:18
  254.4 89.8 %copy-start.4 = (bf16[512,1024]{1,0:T(8,128)(2,1)S(1)}, bf16[512,1024]{1,0:T(8,128)(2,1)}, u32[]{:S(2)}) copy-start(bf16[512,1024]{1,0:T(8,128)(2,1)} %all-gather.17.cloned.1.call-done) | copy-start | bytes 3145732
Sparse Core Ops, SparseCore 0:
  10.4 19.3 all-gather.8
  31.9 43.4 all-gather.10
  77.4 42.1 all-gather.12
  121.6 42.1 all-gather.14
  168.7 23.4 reduce-scatter.2
  194.0 43.4 all-gather.18
  239.1 15.3 all-gather.16
  256.5 43.4 all-gather.20
  302.0 42.1 all-gather.22
  349.1 23.4 reduce-scatter.4
where the time goes:
time: 383 us; the launch traced here: 382 us
  waiting for transfers between devices  344 us (90%)
  matrix products  14.7 us (4%)
  between operations  13.6 us (4%)
  other arithmetic  9.24 us (2%)
    all_gather x2, waiting for transfers between devices, collect_weights(): down_full = lax.all_gather(down_local, 'fs', axis=1, tiled=True)  88.4 us
    all_gather x2, waiting for transfers between devices, collect_weights(): lax.all_gather(gate_local, 'fs', axis=0, tiled=True)  86.1 us
    all_gather x2, waiting for transfers between devices, collect_weights(): lax.all_gather(up_local, 'fs', axis=0, tiled=True)  84.5 us
    reduce_scatter x2, waiting for transfers between devices, summed_rows(): lax.psum_scatter(sent, axis, scatter_dimension=0, tiled=True)  46.4 us
    all_gather x2, waiting for transfers between devices, over_all(): everything = lax.all_gather(section, axis, axis=dim, tiled=True)  34.3 us
    dot_general x2, matrix products, project(): return jnp.dot(row_block, down_full, preferred_element_type=jnp.float32)  9.42 us
  transfers between devices with their start and end apart: 10, of which 10 were waited for; matrix products, arithmetic and copies ran while one was open for 2% of the time, Pallas kernels for 0%

commit v1 on v0

v1 whole, which is shorter than its diff:
```python
import functools
import math

import jax
import jax.numpy as jnp
from jax import lax
from jax.experimental import pallas as pl
from jax.experimental.pallas import tpu as pltpu
from jax.sharding import PartitionSpec as P

epsilon = 1e-06
half_weight = 0.5
CORES = 2
PAIR = 2
MESH = pl.DeviceIdType.MESH


def rms_rows(values, gain_row):
    widened = values.astype(jnp.float32)
    inverse_rms = lax.rsqrt(jnp.mean(widened * widened, axis=-1, keepdims=True) + epsilon)
    return (widened * inverse_rms * gain_row).astype(jnp.bfloat16)


def add_branch(rows, normed_branch, factor):
    return (rows.astype(jnp.float32) + factor * normed_branch.astype(jnp.float32)).astype(
        jnp.bfloat16
    )


def layer_kernel(
    dims,
    stream_ref, mixer_ref, gains_ref, mixer_gain_ref, gu1_ref, d1_ref, gu2_ref, d2_ref,
    out_ref,
    gu_all, dn_all, tok, hid, part, psend, rcore, sums, rx, up_sum, rp, mixed,
    zs, zr, ys, yr, gps, gpr, gxs, gxr, gcs, gcr, rcs, rcr, rxs, rxr, rps, rpr, loc,
):
    Z, Y, X, PP, H, HP = dims
    rows = stream_ref.shape[0]
    f, t = lax.axis_index("fs"), lax.axis_index("tp")
    z, y = f // Y, f % Y
    x, c = t // CORES, t % CORES
    p, q = z % PP, z // PP
    gu_in, d_in = (gu1_ref, gu2_ref), (d1_ref, d2_ref)
    alls = (gu_all, dn_all)
    ins = (gu_in, d_in)

    def fs_of(z_to, y_to):
        return z_to * Y + y_to

    def p_peer(kp):
        return (fs_of(q * PP + (p + kp) % PP, y), t)

    def x_peer(kx):
        return (f, ((x + kx) % X) * CORES + c)

    sibling = (f, x * CORES + 1 - c)
    sent = []

    def send(src, dst, s_sem, r_sem, device):
        d = pltpu.make_async_remote_copy(
            src_ref=src, dst_ref=dst, send_sem=s_sem, recv_sem=r_sem,
            device_id=device, device_id_type=MESH,
        )
        d.start()
        sent.append(d)

    def arrived(dst, s_sem, r_sem):
        pltpu.make_async_remote_copy(
            src_ref=dst, dst_ref=dst, send_sem=s_sem, recv_sem=r_sem,
            device_id=sibling, device_id_type=MESH,
        ).wait_recv()

    barrier = pltpu.get_barrier_semaphore()
    peers = [(fs_of((z + k) % Z, y), t) for k in range(1, Z)]
    peers += [(fs_of(z, (y + j) % Y), t) for j in range(1, Y)]
    peers += [x_peer(k) for k in range(1, X)] + [sibling]
    for peer in peers:
        pl.semaphore_signal(barrier, inc=1, device_id=peer, device_id_type=MESH)
    pl.semaphore_wait(barrier, len(peers))

    def z_send(layer, kind):
        for k in range(1, Z):
            dz = (z + k) % Z
            send(ins[kind][layer].at[dz % PP], alls[kind].at[layer, f],
                 zs.at[layer, kind, k], zr.at[layer, kind, k], (fs_of(dz, y), t))

    def y_send(layer, kind, k):
        slot = fs_of((z - k + Z) % Z, y)
        src = ins[kind][layer].at[p] if k == 0 else alls[kind].at[layer, slot]
        if k:
            arrived(alls[kind].at[layer, slot], zs.at[layer, kind, k], zr.at[layer, kind, k])
        for j in range(1, Y):
            send(src, alls[kind].at[layer, slot],
                 ys.at[layer, kind, k, j], yr.at[layer, kind, k, j],
                 (fs_of(z, (y + j) % Y), t))

    def y_wait(layer, kind):
        for k in range(Z):
            for j in range(1, Y):
                slot = fs_of((z - k + Z) % Z, (y - j + Y) % Y)
                arrived(alls[kind].at[layer, slot],
                        ys.at[layer, kind, k, j], yr.at[layer, kind, k, j])

    def forward(layer, kind):
        for k in range(1, Z):
            y_send(layer, kind, k)

    locals_ = []
    for layer in range(2):
        for kind in range(2):
            d = pltpu.make_async_copy(ins[kind][layer].at[p], alls[kind].at[layer, f],
                                      loc.at[layer, kind])
            d.start()
            locals_.append(d)

    def tok_at(phase, kp, kx, core):
        g = (((p - kp + PP) % PP) * X + (x - kx + X) % X) * CORES + core
        return tok.at[phase, pl.ds(pl.multiple_of(g * rows, rows), rows)]

    def gather_x(phase, kp):
        for kx in range(1, X):
            send(tok_at(phase, kp, 0, c), tok_at(phase, kp, 0, c),
                 gxs.at[phase, kp, kx], gxr.at[phase, kp, kx], x_peer(kx))

    def gather_c(phase, kp, kx):
        send(tok_at(phase, kp, kx, c), tok_at(phase, kp, kx, c),
             gcs.at[phase, kp, kx], gcr.at[phase, kp, kx], sibling)

    def gather_start(phase):
        for kp in range(1, PP):
            send(tok_at(phase, 0, 0, c), tok_at(phase, 0, 0, c),
                 gps.at[phase, kp], gpr.at[phase, kp], p_peer(kp))
        gather_x(phase, 0)
        gather_c(phase, 0, 0)

    def gather_relay(phase):
        for kp in range(1, PP):
            arrived(tok_at(phase, kp, 0, c), gps.at[phase, kp], gpr.at[phase, kp])
            gather_x(phase, kp)
            gather_c(phase, kp, 0)

    def gather_cross(phase):
        for kp in range(PP):
            for kx in range(1, X):
                arrived(tok_at(phase, kp, kx, c),
                        gxs.at[phase, kp, kx], gxr.at[phase, kp, kx])
                gather_c(phase, kp, kx)

    def gather_end(phase):
        for kp in range(PP):
            for kx in range(X):
                arrived(tok_at(phase, kp, kx, 1 - c),
                        gcs.at[phase, kp, kx], gcr.at[phase, kp, kx])

    both = CORES * rows

    def gate_up(layer):
        def step(i, carry):
            at = pl.ds(pl.multiple_of(i * both, both), both)
            weights = gu_all[layer].reshape(-1, 2 * HP)
            gu = jnp.dot(tok[layer, at, :], weights, preferred_element_type=jnp.float32)
            gate, value = gu[:, :HP], gu[:, HP:]
            hid[at, :] = (gate / (1.0 + jnp.exp(-gate)) * value).astype(jnp.bfloat16)
            return carry
        lax.fori_loop(0, PP * X, step, 0)

    order = [(kp, kx) for kp in reversed(range(PP)) for kx in reversed(range(X))]

    def project(layer):
        for kp, kx in order:
            o = kp * X + kx
            i = ((p + kp) % PP) * X + (x + kx) % X
            block = hid[pl.ds(pl.multiple_of(i * both, both), both), :][:, :H]
            down = jnp.concatenate([dn_all[layer, s] for s in range(Z * Y)], axis=1)
            res = jnp.dot(block, down, preferred_element_type=jnp.float32)
            low, high = res[:rows], res[rows:]
            part[o] = jnp.where(c == 0, low, high)
            psend[layer, o] = jnp.where(c == 0, high, low).astype(jnp.bfloat16)
            send(psend.at[layer, o], rcore.at[layer, o], rcs.at[layer, o], rcr.at[layer, o],
                 sibling)

    def reduce_core(layer):
        for kp, kx in order:
            o = kp * X + kx
            arrived(rcore.at[layer, o], rcs.at[layer, o], rcr.at[layer, o])
            total = part[o] + rcore[layer, o].astype(jnp.float32)
            if kx == 0:
                part[o] = total
            else:
                sums[layer, o] = total.astype(jnp.bfloat16)
                send(sums.at[layer, o], rx.at[layer, o], rxs.at[layer, o], rxr.at[layer, o],
                     x_peer(kx))

    def reduce_x(layer):
        for kp in reversed(range(PP)):
            total = part[kp * X]
            for kx in range(1, X):
                o = kp * X + kx
                arrived(rx.at[layer, o], rxs.at[layer, o], rxr.at[layer, o])
                total = total + rx[layer, o].astype(jnp.float32)
            if kp == 0:
                part[0] = total
            else:
                up_sum[layer, kp] = total.astype(jnp.bfloat16)
                send(up_sum.at[layer, kp], rp.at[layer, kp], rps.at[layer, kp],
                     rpr.at[layer, kp], p_peer(kp))

    def reduce_p(layer):
        total = part[0]
        for kp in range(1, PP):
            arrived(rp.at[layer, kp], rps.at[layer, kp], rpr.at[layer, kp])
            total = total + rp[layer, kp].astype(jnp.float32)
        return total.astype(jnp.bfloat16)

    own_rows = pl.ds(pl.multiple_of(((p * X + x) * CORES + c) * rows, rows), rows)

    z_send(0, 0)
    y_send(0, 0, 0)
    tok[0, own_rows, :] = rms_rows(stream_ref[...], gains_ref[0:1, :])
    gather_start(0)
    z_send(0, 1)
    y_send(0, 1, 0)
    gather_relay(0)
    forward(0, 0)
    gather_cross(0)
    z_send(1, 0)
    y_send(1, 0, 0)
    for d in locals_:
        d.wait()
    gather_end(0)
    forward(0, 1)
    y_wait(0, 0)
    gate_up(0)
    y_wait(0, 1)
    project(0)
    reduce_core(0)
    reduce_x(0)
    z_send(1, 1)
    y_send(1, 1, 0)
    branch = reduce_p(0)
    after_first = add_branch(
        stream_ref[...], rms_rows(branch, gains_ref[1:2, :]), half_weight
    )
    joined = add_branch(after_first, rms_rows(mixer_ref[...], mixer_gain_ref[...]), 1.0)
    mixed[...] = joined
    tok[1, own_rows, :] = rms_rows(joined, gains_ref[2:3, :])
    gather_start(1)
    gather_relay(1)
    forward(1, 0)
    gather_cross(1)
    gather_end(1)
    forward(1, 1)
    y_wait(1, 0)
    gate_up(1)
    y_wait(1, 1)
    project(1)
    reduce_core(1)
    reduce_x(1)
    branch_two = reduce_p(1)
    out_ref[...] = add_branch(
        mixed[...], rms_rows(branch_two, gains_ref[3:4, :]), half_weight
    )
    for d in sent:
        d.wait_send()


def on_device(sizes, stream, mixer_out, ffn_gains, mixer_gain,
              gate_first, up_first, down_first, gate_second, up_second, down_second):
    n_fs, n_tp = sizes
    X = n_tp // CORES
    Y = math.gcd(n_fs, X)
    Z = n_fs // Y
    PP = math.gcd(Z, PAIR)
    depth, local_h = gate_first.shape
    H = local_h // PP
    HP = -(-H // 128) * 128
    rows, width = stream.shape

    def halves(gate, up):
        def cut(w):
            w = w.reshape(depth, PP, H).transpose(1, 0, 2)
            return jnp.pad(w, ((0, 0), (0, 0), (0, HP - H)))
        return jnp.concatenate([cut(gate), cut(up)], axis=2)

    def rows_cut(down):
        return down.reshape(PP, H, down.shape[1])

    group = PP * X
    bf, f32 = jnp.bfloat16, jnp.float32
    dma = pltpu.SemaphoreType.DMA
    vm = pltpu.VMEM
    F = n_fs
    scratch = [
        vm((2, F, depth, 2 * HP), bf), vm((2, F, H, depth), bf),
        vm((2, group * CORES * rows, width), bf), vm((group * CORES * rows, HP), bf),
        vm((group, rows, width), f32), vm((2, group, rows, width), bf),
        vm((2, group, rows, width), bf), vm((2, group, rows, width), bf),
        vm((2, group, rows, width), bf), vm((2, PP, rows, width), bf),
        vm((2, PP, rows, width), bf), vm((rows, width), bf),
        dma((2, 2, Z)), dma((2, 2, Z)), dma((2, 2, Z, Y)), dma((2, 2, Z, Y)),
        dma((2, PP)), dma((2, PP)), dma((2, PP, X)), dma((2, PP, X)),
        dma((2, PP, X)), dma((2, PP, X)), dma((2, group)), dma((2, group)),
        dma((2, group)), dma((2, group)), dma((2, PP)), dma((2, PP)), dma((2, 2)),
    ]
    return pl.pallas_call(
        functools.partial(layer_kernel, (Z, Y, X, PP, H, HP)),
        out_shape=jax.ShapeDtypeStruct((rows, width), bf),
        in_specs=[pl.BlockSpec(memory_space=vm)] * 8,
        out_specs=pl.BlockSpec(memory_space=vm),
        scratch_shapes=scratch,
        compiler_params=pltpu.CompilerParams(collective_id=0, has_side_effects=True),
        name="macaron",
    )(stream, mixer_out, ffn_gains, mixer_gain.reshape(1, -1),
      halves(gate_first, up_first), rows_cut(down_first),
      halves(gate_second, up_second), rows_cut(down_second))


def solution(mesh):
    in_specs = (
        P(("fs", "tp"), None), P(("fs", "tp"), None), P(), P(),
        P("fs", "tp"), P("fs", "tp"), P("tp", "fs"),
        P("fs", "tp"), P("fs", "tp"), P("tp", "fs"),
    )
    sizes = (mesh.shape["fs"], mesh.shape["tp"])
    return jax.shard_map(
        functools.partial(on_device, sizes), mesh=mesh, in_specs=in_specs,
        out_specs=P(("fs", "tp"), None), check_vma=False,
    )
```

time: 383 us -> 125 us (0.33)
  waiting for transfers between devices: 344 us -> 0 us
  Pallas kernels: 0 us -> 119 us
  matrix products: 14.7 us -> 0 us
  between operations: 13.6 us -> 0.04 us
  other arithmetic: 9.24 us -> 0.98 us
  local copies, waits for them, and re-layouts: 0.9 us -> 4.8 us
    all_gather x8 -> x0, waiting for transfers between devices: 293 us -> none  [the longest x2 88.4 us: collect_weights(): down_full = lax.all_gather(down_local, 'fs', axis=1, tiled=True)]
    pallas_call x0 -> x1, Pallas kernels: none -> 119 us  [on_device(): pl.pallas_call(functools.partial(layer_kernel, (Z, Y, X, PP, H, HP)), out...]
    reduce_scatter x2 -> x0, waiting for transfers between devices: 46.4 us -> none  [summed_rows(): lax.psum_scatter(sent, axis, scatter_dimension=0, tiled=True)]
    dot_general x4 -> x0, matrix products: 14.7 us -> none  [the longest x2 9.42 us: project(): return jnp.dot(row_block, down_full, preferred_element_type=jnp.float32)]
    reduce_sum x5 -> x0, other arithmetic: 4.73 us -> none  [rms_rows(): jnp.mean(widened * widened, axis=-1, keepdims=True) + epsilon]
    convert_element_type x3 -> x0, other arithmetic: 4.47 us -> none  [the longest x2 2.63 us: rms_rows(): (widened * inverse_rms * gain_row.astype(jnp.float32)).astype(jnp.bfloat16)]
    unnamed x10 -> x0, waiting for transfers between devices: 3.86 us -> none
  transfers between devices with their start and end apart: 10 -> 0, of which waited for: 10 -> 0; matrix products, arithmetic and copies ran while one was open for 2% -> 0% of each run, Pallas kernels for 0% -> 0%
where the time goes in v1:
time: 125 us
  Pallas kernels  119 us (95%)
  local copies, waits for them, and re-layouts  4.8 us (4%)
    pallas_call x1, Pallas kernels, on_device(): pl.pallas_call(functools.partial(layer_kernel, (Z, Y, X, PP, H, HP)), out...  119 us
    unnamed x7, local copies, waits for them, and re-layouts  3.16 us

profile of v1, /device:TPU:0, one launch (start us, length us, event | category | flops | bytes accessed | tf_op | source)
XLA Modules:
  0.0 124.9 jit_solution(16155240986512920127)
XLA Ops:
  0.0 0.0 copy-start
  0.0 1.1 copy.11
  1.1 0.0 copy-done
  1.1 0.0 copy-start.1
  1.1 0.2 copy.12
  1.3 0.7 copy-done.1
  2.1 0.0 copy-start.2
  2.1 0.2 copy.13
  2.2 0.7 copy-done.2
  3.0 0.2 copy.14
  3.2 1.0 fusion.4
  4.1 119.1 %macaron.1 = bf16[128,1024]{1,0:T(8,128)(2,1)} custom-call(bf16[128,1024]{1,0:T(8,128)(2,1)} %stream_ref.1, bf16[128,1024]{1,0:T(8,128)(2,1)} %mixer_ref.1, f32[4,1024]{1,0:T(4,128)} %gains_ref.1, f32[1,1024]{1,0:T(1,128)} %bitcast.21, bf16[2,128,768]{2,1,0:T(8,128)(2,1)} %get-tuple-element.5.gu1_ref, bf16[2,352,128]{2,1,0:T(8,128)(2,1)} %bitcast.19, ...), custom_call_target="tpu_custom_call" | custom-call | tf_op jit(solution)/shard_map/macaron/pallas_call | solution.py:305
  123.2 1.7 %copy.16 = bf16[128,1024]{1,0:T(8,128)(2,1)} copy(bf16[128,1024]{1,0:T(8,128)(2,1)} %macaron.1) | data formatting | bytes 524288
Async XLA Ops:
  0.0 1.1 copy-start
  1.1 0.9 copy-start.1
  2.1 0.9 copy-start.2

commit v2 on v1

--- a/solution.py
+++ b/solution.py
@@ -29,20 +29,45 @@
 
 def layer_kernel(
     dims,
-    stream_ref, mixer_ref, gains_ref, mixer_gain_ref, gu1_ref, d1_ref, gu2_ref, d2_ref,
+    stream_hbm, mixer_hbm, gains_ref, mixer_gain_ref,
+    g1_hbm, u1_hbm, d1_ref, g2_hbm, u2_hbm, d2_ref,
     out_ref,
-    gu_all, dn_all, tok, hid, part, psend, rcore, sums, rx, up_sum, rp, mixed,
-    zs, zr, ys, yr, gps, gpr, gxs, gxr, gcs, gcr, rcs, rcr, rxs, rxr, rps, rpr, loc,
+    stream_ref, mixer_ref, raw, gu_in, gu_all, dn_all, tok, hid, part, psend, rcore, sums, rx, up_sum, rp, mixed,
+    zs, zr, ys, yr, gps, gpr, gxs, gxr, gcs, gcr, rcs, rcr, rxs, rxr, rps, rpr, loc, lin,
 ):
     Z, Y, X, PP, H, HP = dims
     rows = stream_ref.shape[0]
+    depth = raw.shape[2]
     f, t = lax.axis_index("fs"), lax.axis_index("tp")
     z, y = f // Y, f % Y
     x, c = t // CORES, t % CORES
     p, q = z % PP, z // PP
-    gu_in, d_in = (gu1_ref, gu2_ref), (d1_ref, d2_ref)
+    d_in = (d1_ref, d2_ref)
     alls = (gu_all, dn_all)
-    ins = (gu_in, d_in)
+
+    def half_of(kind, layer, which):
+        if kind == 0:
+            return gu_in.at[layer, which]
+        return d_in[layer].at[pl.ds(pl.multiple_of(which * H, 16), H)]
+
+    loads = []
+    for n, (src, dst) in enumerate((
+        (stream_hbm, stream_ref), (g1_hbm, raw.at[0, 0]), (u1_hbm, raw.at[0, 1]),
+        (g2_hbm, raw.at[1, 0]), (u2_hbm, raw.at[1, 1]), (mixer_hbm, mixer_ref),
+    )):
+        d = pltpu.make_async_copy(src, dst, lin.at[n])
+        d.start()
+        loads.append(d)
+
+    def pack(layer):
+        fill = jnp.zeros((depth, HP - H), jnp.bfloat16)
+        for side in range(2):
+            w = raw[layer, side]
+            for which in range(PP):
+                cut = w[:, which * H:(which + 1) * H]
+                if HP > H:
+                    cut = jnp.concatenate([cut, fill], axis=1)
+                gu_in[layer, which, :, side * HP:(side + 1) * HP] = cut
 
     def fs_of(z_to, y_to):
         return z_to * Y + y_to
@@ -81,12 +106,12 @@
     def z_send(layer, kind):
         for k in range(1, Z):
             dz = (z + k) % Z
-            send(ins[kind][layer].at[dz % PP], alls[kind].at[layer, f],
+            send(half_of(kind, layer, dz % PP), alls[kind].at[layer, f],
                  zs.at[layer, kind, k], zr.at[layer, kind, k], (fs_of(dz, y), t))
 
     def y_send(layer, kind, k):
         slot = fs_of((z - k + Z) % Z, y)
-        src = ins[kind][layer].at[p] if k == 0 else alls[kind].at[layer, slot]
+        src = half_of(kind, layer, p) if k == 0 else alls[kind].at[layer, slot]
         if k:
             arrived(alls[kind].at[layer, slot], zs.at[layer, kind, k], zr.at[layer, kind, k])
         for j in range(1, Y):
@@ -106,9 +131,10 @@
             y_send(layer, kind, k)
 
     locals_ = []
-    for layer in range(2):
+
+    def keep_own(layer):
         for kind in range(2):
-            d = pltpu.make_async_copy(ins[kind][layer].at[p], alls[kind].at[layer, f],
+            d = pltpu.make_async_copy(half_of(kind, layer, p), alls[kind].at[layer, f],
                                       loc.at[layer, kind])
             d.start()
             locals_.append(d)
@@ -214,29 +240,41 @@
 
     own_rows = pl.ds(pl.multiple_of(((p * X + x) * CORES + c) * rows, rows), rows)
 
+    loads[0].wait()
+    tok[0, own_rows, :] = rms_rows(stream_ref[...], gains_ref[0:1, :])
+    gather_start(0)
+    loads[1].wait()
+    loads[2].wait()
+    pack(0)
     z_send(0, 0)
     y_send(0, 0, 0)
-    tok[0, own_rows, :] = rms_rows(stream_ref[...], gains_ref[0:1, :])
-    gather_start(0)
     z_send(0, 1)
     y_send(0, 1, 0)
+    keep_own(0)
+    loads[3].wait()
+    loads[4].wait()
+    pack(1)
+    z_send(1, 0)
+    z_send(1, 1)
+    keep_own(1)
     gather_relay(0)
+    gather_cross(0)
     forward(0, 0)
-    gather_cross(0)
-    z_send(1, 0)
+    gather_end(0)
+    forward(0, 1)
     y_send(1, 0, 0)
+    y_send(1, 1, 0)
+    loads[5].wait()
     for d in locals_:
         d.wait()
-    gather_end(0)
-    forward(0, 1)
     y_wait(0, 0)
     gate_up(0)
     y_wait(0, 1)
     project(0)
     reduce_core(0)
+    forward(1, 0)
     reduce_x(0)
-    z_send(1, 1)
-    y_send(1, 1, 0)
+    forward(1, 1)
     branch = reduce_p(0)
     after_first = add_branch(
         stream_ref[...], rms_rows(branch, gains_ref[1:2, :]), half_weight
@@ -246,10 +284,8 @@
     tok[1, own_rows, :] = rms_rows(joined, gains_ref[2:3, :])
     gather_start(1)
     gather_relay(1)
-    forward(1, 0)
     gather_cross(1)
     gather_end(1)
-    forward(1, 1)
     y_wait(1, 0)
     gate_up(1)
     y_wait(1, 1)
@@ -276,21 +312,15 @@
     HP = -(-H // 128) * 128
     rows, width = stream.shape
 
-    def halves(gate, up):
-        def cut(w):
-            w = w.reshape(depth, PP, H).transpose(1, 0, 2)
-            return jnp.pad(w, ((0, 0), (0, 0), (0, HP - H)))
-        return jnp.concatenate([cut(gate), cut(up)], axis=2)
-
-    def rows_cut(down):
-        return down.reshape(PP, H, down.shape[1])
-
     group = PP * X
     bf, f32 = jnp.bfloat16, jnp.float32
     dma = pltpu.SemaphoreType.DMA
     vm = pltpu.VMEM
     F = n_fs
+    any_ = pl.ANY
     scratch = [
+        vm((rows, width), bf), vm((rows, width), bf), vm((2, 2, depth, local_h), bf),
+        vm((2, PP, depth, 2 * HP), bf),
         vm((2, F, depth, 2 * HP), bf), vm((2, F, H, depth), bf),
         vm((2, group * CORES * rows, width), bf), vm((group * CORES * rows, HP), bf),
         vm((group, rows, width), f32), vm((2, group, rows, width), bf),
@@ -300,19 +330,18 @@
         dma((2, 2, Z)), dma((2, 2, Z)), dma((2, 2, Z, Y)), dma((2, 2, Z, Y)),
         dma((2, PP)), dma((2, PP)), dma((2, PP, X)), dma((2, PP, X)),
         dma((2, PP, X)), dma((2, PP, X)), dma((2, group)), dma((2, group)),
-        dma((2, group)), dma((2, group)), dma((2, PP)), dma((2, PP)), dma((2, 2)),
+        dma((2, group)), dma((2, group)), dma((2, PP)), dma((2, PP)), dma((2, 2)), dma((6,)),
     ]
     return pl.pallas_call(
         functools.partial(layer_kernel, (Z, Y, X, PP, H, HP)),
         out_shape=jax.ShapeDtypeStruct((rows, width), bf),
-        in_specs=[pl.BlockSpec(memory_space=vm)] * 8,
+        in_specs=[pl.BlockSpec(memory_space=m) for m in (any_, any_, vm, vm) + (any_,) * 6],
         out_specs=pl.BlockSpec(memory_space=vm),
         scratch_shapes=scratch,
         compiler_params=pltpu.CompilerParams(collective_id=0, has_side_effects=True),
         name="macaron",
     )(stream, mixer_out, ffn_gains, mixer_gain.reshape(1, -1),
-      halves(gate_first, up_first), rows_cut(down_first),
-      halves(gate_second, up_second), rows_cut(down_second))
+      gate_first, up_first, down_first, gate_second, up_second, down_second)
 
 
 def solution(mesh):

time: 125 us -> 109 us (0.87)
  Pallas kernels: 119 us -> 102 us
  local copies, waits for them, and re-layouts: 4.8 us -> 6.11 us
    pallas_call x1, Pallas kernels: 119 us -> 102 us  [on_device(): pl.pallas_call(functools.partial(layer_kernel, (Z, Y, X, PP, H, HP)), out...]
    unnamed x7 -> x11, local copies, waits for them, and re-layouts: 3.16 us -> 6.11 us
    reshape x4 -> x0, local copies, waits for them, and re-layouts: 1.64 us -> none  [cut(): w = w.reshape(depth, PP, H).transpose(1, 0, 2)]
where the time goes in v2:
time: 109 us; the launch traced here: 108 us
  Pallas kernels  102 us (94%)
  local copies, waits for them, and re-layouts  6.11 us (6%)
    pallas_call x1, Pallas kernels, on_device(): pl.pallas_call(functools.partial(layer_kernel, (Z, Y, X, PP, H, HP)), out...  102 us
    unnamed x11, local copies, waits for them, and re-layouts  6.11 us

profile of v2, /device:TPU:0, one launch (start us, length us, event | category | flops | bytes accessed | tf_op | source)
XLA Modules:
  0.0 108.2 jit_solution(11974888150072175813)
XLA Ops:
  0.0 0.0 copy-start
  0.0 1.8 %copy.11.g1_hbm = bf16[128,704]{1,0:T(8,128)(2,1)} copy(bf16[128,704]{0,1:T(8,128)(2,1)} %param.14) | data formatting | bytes 360448 | tf_op args[4]
  1.8 0.0 copy-done
  1.8 0.0 copy-start.1
  1.8 0.8 copy.12.u1_hbm
  2.6 0.1 copy-done.1
  2.7 0.0 copy-start.2
  2.7 0.8 copy.13.g2_hbm
  3.5 0.1 copy-done.2
  3.6 0.8 copy.14.u2_hbm
  4.4 102.1 %macaron.1 = bf16[128,1024]{1,0:T(8,128)(2,1)} custom-call(bf16[128,1024]{1,0:T(8,128)(2,1)} %stream_hbm.1, bf16[128,1024]{1,0:T(8,128)(2,1)} %mixer_hbm.1, f32[4,1024]{1,0:T(4,128)} %gains_ref.1, f32[1,1024]{1,0:T(1,128)} %bitcast.1, bf16[128,704]{1,0:T(8,128)(2,1)} %copy.11.g1_hbm, bf16[128,704]{1,0:T(8,128)(2,1)} %copy.12.u1_hbm, ...), custom_call_target="tpu_custom_call" | custom-call | tf_op jit(solution)/shard_map/macaron/pallas_call | solution.py:335
  106.6 1.7 %copy.16 = bf16[128,1024]{1,0:T(8,128)(2,1)} copy(bf16[128,1024]{1,0:T(8,128)(2,1)} %macaron.1) | data formatting | bytes 524288
Async XLA Ops:
  0.0 1.8 %copy-start = (bf16[128,704]{0,1:T(8,128)(2,1)S(1)}, bf16[128,704]{0,1:T(8,128)(2,1)}, u32[]{:S(2)}) copy-start(bf16[128,704]{0,1:T(8,128)(2,1)} %param.15) | copy-start | bytes 540676
  1.8 0.9 copy-start.1
  2.7 0.9 copy-start.2

commit v3 on v2

--- a/solution.py
+++ b/solution.py
@@ -139,104 +139,166 @@
             d.start()
             locals_.append(d)
 
-    def tok_at(phase, kp, kx, core):
+    half = rows // 2
+
+    def tok_at(phase, h, kp, kx, core):
         g = (((p - kp + PP) % PP) * X + (x - kx + X) % X) * CORES + core
-        return tok.at[phase, pl.ds(pl.multiple_of(g * rows, rows), rows)]
-
-    def gather_x(phase, kp):
+        return tok.at[phase, pl.ds(pl.multiple_of(g * rows + h * half, half), half)]
+
+    def gather_x(phase, h, kp):
         for kx in range(1, X):
-            send(tok_at(phase, kp, 0, c), tok_at(phase, kp, 0, c),
-                 gxs.at[phase, kp, kx], gxr.at[phase, kp, kx], x_peer(kx))
-
-    def gather_c(phase, kp, kx):
-        send(tok_at(phase, kp, kx, c), tok_at(phase, kp, kx, c),
-             gcs.at[phase, kp, kx], gcr.at[phase, kp, kx], sibling)
+            send(tok_at(phase, h, kp, 0, c), tok_at(phase, h, kp, 0, c),
+                 gxs.at[phase, h, kp, kx], gxr.at[phase, h, kp, kx], x_peer(kx))
+
+    def gather_p(phase, h, kx):
+        for kp in range(1, PP):
+            send(tok_at(phase, h, 0, kx, c), tok_at(phase, h, 0, kx, c),
+                 gps.at[phase, h, kp, kx], gpr.at[phase, h, kp, kx], p_peer(kp))
+
+    def gather_c(phase, h, kp, kx):
+        send(tok_at(phase, h, kp, kx, c), tok_at(phase, h, kp, kx, c),
+             gcs.at[phase, h, kp, kx], gcr.at[phase, h, kp, kx], sibling)
+
+    def got_x(phase, h, kp, kx):
+        arrived(tok_at(phase, h, kp, kx, c), gxs.at[phase, h, kp, kx],
+                gxr.at[phase, h, kp, kx])
+
+    def got_p(phase, h, kp, kx):
+        arrived(tok_at(phase, h, kp, kx, c), gps.at[phase, h, kp, kx],
+                gpr.at[phase, h, kp, kx])
+
+    def p_first(phase):
+        return (0,) if phase else (0, 1)
+
+    def x_first(phase):
+        return (1,) if phase else ()
 
     def gather_start(phase):
-        for kp in range(1, PP):
-            send(tok_at(phase, 0, 0, c), tok_at(phase, 0, 0, c),
-                 gps.at[phase, kp], gpr.at[phase, kp], p_peer(kp))
-        gather_x(phase, 0)
-        gather_c(phase, 0, 0)
+        for h in p_first(phase):
+            gather_p(phase, h, 0)
+        for h in x_first(phase):
+            gather_x(phase, h, 0)
+            gather_p(phase, h, 0)
+        for h in p_first(phase):
+            gather_x(phase, h, 0)
+        for h in range(2):
+            gather_c(phase, h, 0, 0)
 
     def gather_relay(phase):
-        for kp in range(1, PP):
-            arrived(tok_at(phase, kp, 0, c), gps.at[phase, kp], gpr.at[phase, kp])
-            gather_x(phase, kp)
-            gather_c(phase, kp, 0)
+        for h in x_first(phase):
+            for kx in range(1, X):
+                got_x(phase, h, 0, kx)
+                gather_p(phase, h, kx)
+                gather_c(phase, h, 0, kx)
+        for h in p_first(phase):
+            for kp in range(1, PP):
+                got_p(phase, h, kp, 0)
+                gather_x(phase, h, kp)
+                gather_c(phase, h, kp, 0)
 
     def gather_cross(phase):
-        for kp in range(PP):
-            for kx in range(1, X):
-                arrived(tok_at(phase, kp, kx, c),
-                        gxs.at[phase, kp, kx], gxr.at[phase, kp, kx])
-                gather_c(phase, kp, kx)
+        for h in p_first(phase):
+            for kp in range(PP):
+                for kx in range(1, X):
+                    got_x(phase, h, kp, kx)
+                    gather_c(phase, h, kp, kx)
+        for h in x_first(phase):
+            for kx in range(X):
+                for kp in range(1, PP):
+                    got_p(phase, h, kp, kx)
+                    gather_c(phase, h, kp, kx)
 
     def gather_end(phase):
-        for kp in range(PP):
-            for kx in range(X):
-                arrived(tok_at(phase, kp, kx, 1 - c),
-                        gcs.at[phase, kp, kx], gcr.at[phase, kp, kx])
+        for h in range(2):
+            for kp in range(PP):
+                for kx in range(X):
+                    arrived(tok_at(phase, h, kp, kx, 1 - c),
+                            gcs.at[phase, h, kp, kx], gcr.at[phase, h, kp, kx])
 
     both = CORES * rows
+    chunk = both * math.gcd(PP * X, 2)
 
     def gate_up(layer):
         def step(i, carry):
-            at = pl.ds(pl.multiple_of(i * both, both), both)
+            at = pl.ds(pl.multiple_of(i * chunk, chunk), chunk)
             weights = gu_all[layer].reshape(-1, 2 * HP)
             gu = jnp.dot(tok[layer, at, :], weights, preferred_element_type=jnp.float32)
             gate, value = gu[:, :HP], gu[:, HP:]
             hid[at, :] = (gate / (1.0 + jnp.exp(-gate)) * value).astype(jnp.bfloat16)
             return carry
-        lax.fori_loop(0, PP * X, step, 0)
-
-    order = [(kp, kx) for kp in reversed(range(PP)) for kx in reversed(range(X))]
+        lax.fori_loop(0, PP * X * both // chunk, step, 0)
+
+    order = sorted(((kp, kx) for kp in range(PP) for kx in range(X)),
+                   key=lambda o: (o[1] == 0, o[0] == 0))
+    top, low_half = pl.ds(0, half), pl.ds(half, half)
+
+    def project_one(layer, kp, kx):
+        o = kp * X + kx
+        i = ((p + kp) % PP) * X + (x + kx) % X
+        block = hid[pl.ds(pl.multiple_of(i * both, both), both), :][:, :H]
+        down = jnp.concatenate([dn_all[layer, s] for s in range(Z * Y)], axis=1)
+        res = jnp.dot(block, down, preferred_element_type=jnp.float32)
+        low, high = res[:rows], res[rows:]
+        part[o] = jnp.where(c == 0, low, high)
+        psend[layer, o] = jnp.where(c == 0, high, low).astype(jnp.bfloat16)
+        send(psend.at[layer, o], rcore.at[layer, o], rcs.at[layer, o], rcr.at[layer, o],
+             sibling)
+
+    def reduce_one(layer, kp, kx):
+        o = kp * X + kx
+        arrived(rcore.at[layer, o], rcs.at[layer, o], rcr.at[layer, o])
+        total = part[o] + rcore[layer, o].astype(jnp.float32)
+        part[o] = total
+        if kp or kx:
+            sums[layer, o] = total.astype(jnp.bfloat16)
+        for h, at in enumerate((top, low_half)):
+            first = kx if h in p_first(layer) else kp
+            if first:
+                send(sums.at[layer, o, at], rx.at[layer, o, at], rxs.at[layer, h, o],
+                     rxr.at[layer, h, o],
+                     x_peer(kx) if h in p_first(layer) else p_peer(kp))
 
     def project(layer):
-        for kp, kx in order:
-            o = kp * X + kx
-            i = ((p + kp) % PP) * X + (x + kx) % X
-            block = hid[pl.ds(pl.multiple_of(i * both, both), both), :][:, :H]
-            down = jnp.concatenate([dn_all[layer, s] for s in range(Z * Y)], axis=1)
-            res = jnp.dot(block, down, preferred_element_type=jnp.float32)
-            low, high = res[:rows], res[rows:]
-            part[o] = jnp.where(c == 0, low, high)
-            psend[layer, o] = jnp.where(c == 0, high, low).astype(jnp.bfloat16)
-            send(psend.at[layer, o], rcore.at[layer, o], rcs.at[layer, o], rcr.at[layer, o],
-                 sibling)
-
-    def reduce_core(layer):
-        for kp, kx in order:
-            o = kp * X + kx
-            arrived(rcore.at[layer, o], rcs.at[layer, o], rcr.at[layer, o])
-            total = part[o] + rcore[layer, o].astype(jnp.float32)
-            if kx == 0:
-                part[o] = total
-            else:
-                sums[layer, o] = total.astype(jnp.bfloat16)
-                send(sums.at[layer, o], rx.at[layer, o], rxs.at[layer, o], rxr.at[layer, o],
-                     x_peer(kx))
+        for n, (kp, kx) in enumerate(order):
+            project_one(layer, kp, kx)
+            if n:
+                reduce_one(layer, *order[n - 1])
+        reduce_one(layer, *order[-1])
+
+    def first_sum(layer, h, at, keep, others):
+        total = part[keep, at, :]
+        for o in others:
+            arrived(rx.at[layer, o, at], rxs.at[layer, h, o], rxr.at[layer, h, o])
+            total = total + rx[layer, o, at, :].astype(jnp.float32)
+        return total
+
+    def second_send(layer, h, at, n, total, device):
+        up_sum[layer, n, at, :] = total.astype(jnp.bfloat16)
+        send(up_sum.at[layer, n, at], rp.at[layer, n, at], rps.at[layer, h, n],
+             rpr.at[layer, h, n], device)
 
     def reduce_x(layer):
-        for kp in reversed(range(PP)):
-            total = part[kp * X]
-            for kx in range(1, X):
-                o = kp * X + kx
-                arrived(rx.at[layer, o], rxs.at[layer, o], rxr.at[layer, o])
-                total = total + rx[layer, o].astype(jnp.float32)
-            if kp == 0:
-                part[0] = total
-            else:
-                up_sum[layer, kp] = total.astype(jnp.bfloat16)
-                send(up_sum.at[layer, kp], rp.at[layer, kp], rps.at[layer, kp],
-                     rpr.at[layer, kp], p_peer(kp))
+        for h, at in enumerate((top, low_half)):
+            straight = h in p_first(layer)
+            for n in reversed(range(PP if straight else X)):
+                if straight:
+                    keep, others = n * X, [n * X + kx for kx in range(1, X)]
+                else:
+                    keep, others = n, [kp * X + n for kp in range(1, PP)]
+                total = first_sum(layer, h, at, keep, others)
+                if n:
+                    second_send(layer, h, at, n, total, p_peer(n) if straight else x_peer(n))
+                else:
+                    part[0, at, :] = total
 
     def reduce_p(layer):
-        total = part[0]
-        for kp in range(1, PP):
-            arrived(rp.at[layer, kp], rps.at[layer, kp], rpr.at[layer, kp])
-            total = total + rp[layer, kp].astype(jnp.float32)
-        return total.astype(jnp.bfloat16)
+        def last(h, at):
+            total = part[0, at, :]
+            for n in range(1, PP if h in p_first(layer) else X):
+                arrived(rp.at[layer, n, at], rps.at[layer, h, n], rpr.at[layer, h, n])
+                total = total + rp[layer, n, at, :].astype(jnp.float32)
+            return total.astype(jnp.bfloat16)
+        return jnp.concatenate([last(0, top), last(1, low_half)], axis=0)
 
     own_rows = pl.ds(pl.multiple_of(((p * X + x) * CORES + c) * rows, rows), rows)
 
@@ -271,7 +333,6 @@
     gate_up(0)
     y_wait(0, 1)
     project(0)
-    reduce_core(0)
     forward(1, 0)
     reduce_x(0)
     forward(1, 1)
@@ -290,7 +351,6 @@
     gate_up(1)
     y_wait(1, 1)
     project(1)
-    reduce_core(1)
     reduce_x(1)
     branch_two = reduce_p(1)
     out_ref[...] = add_branch(
@@ -313,6 +373,7 @@
     rows, width = stream.shape
 
     group = PP * X
+    most = max(PP, X)
     bf, f32 = jnp.bfloat16, jnp.float32
     dma = pltpu.SemaphoreType.DMA
     vm = pltpu.VMEM
@@ -325,12 +386,13 @@
         vm((2, group * CORES * rows, width), bf), vm((group * CORES * rows, HP), bf),
         vm((group, rows, width), f32), vm((2, group, rows, width), bf),
         vm((2, group, rows, width), bf), vm((2, group, rows, width), bf),
-        vm((2, group, rows, width), bf), vm((2, PP, rows, width), bf),
-        vm((2, PP, rows, width), bf), vm((rows, width), bf),
+        vm((2, group, rows, width), bf), vm((2, most, rows, width), bf),
+        vm((2, most, rows, width), bf), vm((rows, width), bf),
         dma((2, 2, Z)), dma((2, 2, Z)), dma((2, 2, Z, Y)), dma((2, 2, Z, Y)),
-        dma((2, PP)), dma((2, PP)), dma((2, PP, X)), dma((2, PP, X)),
-        dma((2, PP, X)), dma((2, PP, X)), dma((2, group)), dma((2, group)),
-        dma((2, group)), dma((2, group)), dma((2, PP)), dma((2, PP)), dma((2, 2)), dma((6,)),
+        dma((2, 2, PP, X)), dma((2, 2, PP, X)), dma((2, 2, PP, X)), dma((2, 2, PP, X)),
+        dma((2, 2, PP, X)), dma((2, 2, PP, X)), dma((2, group)), dma((2, group)),
+        dma((2, 2, group)), dma((2, 2, group)), dma((2, 2, most)), dma((2, 2, most)),
+        dma((2, 2)), dma((6,)),
     ]
     return pl.pallas_call(
         functools.partial(layer_kernel, (Z, Y, X, PP, H, HP)),

time: 109 us -> 100 us (0.917)
  Pallas kernels: 102 us -> 94.1 us
    pallas_call x1, Pallas kernels: 102 us -> 94.1 us  [on_device(): pl.pallas_call(functools.partial(layer_kernel, (Z, Y, X, PP, H, HP)), out...]
where the time goes in v3:
time: 100 us
  Pallas kernels  94.1 us (94%)
  local copies, waits for them, and re-layouts  6.11 us (6%)
    pallas_call x1, Pallas kernels, on_device(): pl.pallas_call(functools.partial(layer_kernel, (Z, Y, X, PP, H, HP)), out...  94.1 us
    unnamed x11, local copies, waits for them, and re-layouts  6.11 us

profile of v3, /device:TPU:0, one launch (start us, length us, event | category | flops | bytes accessed | tf_op | source)
XLA Modules:
  0.0 100.2 jit_solution(6655250539184727294)
XLA Ops:
  0.0 0.0 copy-start
  0.0 1.8 %copy.11.g1_hbm = bf16[128,704]{1,0:T(8,128)(2,1)} copy(bf16[128,704]{0,1:T(8,128)(2,1)} %param.14) | data formatting | bytes 360448 | tf_op args[4]
  1.8 0.0 copy-done
  1.8 0.0 copy-start.1
  1.8 0.8 copy.12.u1_hbm
  2.6 0.1 copy-done.1
  2.7 0.0 copy-start.2
  2.7 0.8 copy.13.g2_hbm
  3.5 0.1 copy-done.2
  3.6 0.8 copy.14.u2_hbm
  4.4 94.1 %macaron.1 = bf16[128,1024]{1,0:T(8,128)(2,1)} custom-call(bf16[128,1024]{1,0:T(8,128)(2,1)} %stream_hbm.1, bf16[128,1024]{1,0:T(8,128)(2,1)} %mixer_hbm.1, f32[4,1024]{1,0:T(4,128)} %gains_ref.1, f32[1,1024]{1,0:T(1,128)} %bitcast.1, bf16[128,704]{1,0:T(8,128)(2,1)} %copy.11.g1_hbm, bf16[128,704]{1,0:T(8,128)(2,1)} %copy.12.u1_hbm, ...), custom_call_target="tpu_custom_call" | custom-call | tf_op jit(solution)/shard_map/macaron/pallas_call | solution.py:397
  98.5 1.7 %copy.16 = bf16[128,1024]{1,0:T(8,128)(2,1)} copy(bf16[128,1024]{1,0:T(8,128)(2,1)} %macaron.1) | data formatting | bytes 524288
Async XLA Ops:
  0.0 1.8 %copy-start = (bf16[128,704]{0,1:T(8,128)(2,1)S(1)}, bf16[128,704]{0,1:T(8,128)(2,1)}, u32[]{:S(2)}) copy-start(bf16[128,704]{0,1:T(8,128)(2,1)} %param.15) | copy-start | bytes 540676
  1.8 0.9 copy-start.1
  2.7 0.9 copy-start.2
